TPU v7x, 32 devices: a whole 2x2x4 slice. The times are simulated.
32 devices in a mesh: sp: 8 (over z, x), tp: 4 (over y, core).
Axes of the slice: x: 2, y: 2, z: 4, core: 2. Of those that a mesh axis runs over, the one named last changes fastest.
Arguments:
- layer_input: bfloat16 [8, 1536, 2048], P('sp', 'tp'), may hold values from -6 to 6
- input_gain: float32 [2048], replicated, may hold values from 0.1 to 1.9
- key_weight: bfloat16 [2048, 512], P('sp', 'tp'), may hold values from -0.125 to 0.125
- value_weight: bfloat16 [2048, 512], P('sp', 'tp'), may hold values from -0.125 to 0.125
- key_gain: float32 [128], replicated, may hold values from 0.1 to 1.9
- stop_shift: bfloat16 [8, 4, 1536], P('sp', None, 'tp'), may hold values from -20 to 0
- new_query: bfloat16 [8, 16, 128], P('sp', 'tp'), may hold values from -6 to 6
- query_gain: float32 [128], replicated, may hold values from 0.1 to 1.9
- out_gain: float32 [128], replicated, may hold values from 0.1 to 1.9
Outputs:
- key_cache: bfloat16 [8, 4, 1536, 128], P('sp', 'tp')
- value_cache: bfloat16 [8, 4, 1536, 128], P('sp', 'tp')
- shift_cache: bfloat16 [8, 4, 1536], P('sp', 'tp')
- first_read: bfloat16 [8, 16, 128], P('sp', 'tp')
All inputs are finite; a program needn't handle non-finite values.
Results may differ from a plain program's by a relative error of at most 0.013.
Values may be sent and summed in bfloat16 or wider, within the bound.
A program may use at most 64 MiB of HBM per device.

v0:
```python
import jax
import jax.numpy as jnp
from jax import lax
from jax.sharding import PartitionSpec as P

KVH = 4
epsilon = 1e-06


def row_norm(value_entries, scaling):
    return (
        value_entries
        * lax.rsqrt(jnp.mean(value_entries * value_entries, axis=-1, keepdims=True) + epsilon)
        * scaling
    )


def shards(
    layer_input,
    input_gain,
    key_weight,
    value_weight,
    key_gain,
    stop_shift,
    new_query,
    query_gain,
    out_gain,
):
    groups = lax.axis_size("tp")
    copies = groups // KVH
    row_count = layer_input.shape[1]
    head_size = new_query.shape[2]
    score_scale = 1.0 / head_size**0.5
    normed = row_norm(layer_input[0].astype(jnp.float32), input_gain).astype(jnp.bfloat16)
    stacked = jnp.stack((key_weight, value_weight), 0)
    full_depth = lax.all_gather(stacked, "sp", axis=1, tiled=True)
    projected = jnp.einsum(
        "rd,kdc->krc",
        normed,
        lax.all_gather(full_depth, "tp", axis=2, tiled=True),
        preferred_element_type=jnp.float32,
    )
    key_rows = row_norm(projected[0].reshape(row_count, KVH, head_size), key_gain).astype(
        jnp.bfloat16
    )
    value_rows = projected[1].reshape(row_count, KVH, head_size).astype(jnp.bfloat16)
    local_shift = stop_shift[0]
    key_slots = jnp.repeat(key_rows, copies, axis=1)
    value_slots = jnp.repeat(value_rows, copies, axis=1)
    shift_slots = jnp.repeat(local_shift.T, copies, axis=1)
    key_got, value_got, shift_got = (
        lax.all_to_all(key_slots, "tp", split_axis=1, concat_axis=0, tiled=True),
        lax.all_to_all(value_slots, "tp", split_axis=1, concat_axis=0, tiled=True),
        lax.all_to_all(shift_slots, "tp", split_axis=1, concat_axis=0, tiled=True),
    )
    key_line = key_got[:, 0, :]
    value_line = value_got[:, 0, :]
    shift_line = shift_got[:, 0]
    length = key_line.shape[0]
    query_rows = row_norm(new_query[0].astype(jnp.float32), query_gain).astype(jnp.bfloat16)
    scores = (
        jnp.einsum("qd,ld->ql", query_rows, key_line, preferred_element_type=jnp.float32)
        * score_scale
    )
    scores = scores + shift_line.astype(jnp.float32)[None, :]
    log_keep = jax.nn.log_sigmoid(-scores)
    inside = lax.cumsum(log_keep, axis=1, reverse=True) - log_keep
    weights = jnp.exp(jax.nn.log_sigmoid(scores) + inside).astype(jnp.bfloat16)
    read_sum = jnp.dot(weights, value_line, preferred_element_type=jnp.float32)
    first_out = row_norm(read_sum, out_gain).astype(jnp.bfloat16)
    return (
        key_line.reshape(1, 1, length, head_size),
        value_line.reshape(1, 1, length, head_size),
        shift_line.reshape(1, 1, length),
        first_out[None],
    )


def solution(mesh):
    placed = (
        P("sp", "tp", None),
        P(),
        P("sp", "tp"),
        P("sp", "tp"),
        P(),
        P("sp", None, "tp"),
        P("sp", "tp", None),
        P(),
        P(),
    )
    return jax.shard_map(
        shards,
        mesh=mesh,
        in_specs=placed,
        out_specs=(
            P("sp", "tp", None, None),
            P("sp", "tp", None, None),
            P("sp", "tp", None),
            P("sp", "tp", None),
        ),
        check_vma=False,
    )
```

profile of v0, /device:TPU:0, one launch (start us, length us, event | category | flops | bytes accessed | tf_op | source)
XLA Modules:
  0.0 125.1 jit_solution(7521093562815016131)
XLA Ops:
  7.2 0.0 copy-start
  7.2 0.0 copy-start.6
  7.2 0.0 all-gather.3.cloned.1.call-start
  7.2 1.0 copy.25
  8.3 0.9 copy.26
  9.2 0.7 pad_maximum_fusion
  9.9 0.0 all-gather.3.cloned.1.call-update
  9.9 0.0 all-gather.5.cloned.1.call-start
  10.0 42.8 %all-gather.3.cloned.1.call-done = bf16[2,2048,128]{1,2,0:T(8,128)(2,1)} async-done(((bf16[2,256,128]{1,2,0:T(8,128)(2,1)}), bf16[2,2048,128]{1,2,0:T(8,128)(2,1)}) %all-gather.3.cloned.1.call-update) | async-done | bytes 1048592 | tf_op jit(solution)/shard_map/all_gather | solution.py:36
  52.8 0.0 all-gather.5.cloned.1.call-update
  52.8 0.7 copy.36
  53.5 0.5 broadcast.75
  54.0 0.7 reduce.5
  54.7 0.7 reshape.96
  55.3 3.2 %all-to-all-start.2 = ((bf16[4,2,192]{2,1,0:T(2,128)(2,1)}), bf16[4,2,192]{2,1,0:T(2,128)(2,1)S(1)}, u32[]{:S(2)}, u32[]{:S(2)}) async-start(bf16[4,2,192]{2,1,0:T(2,128)(2,1)} %reshape.96), calls=%async_computation.2 | async-start | bytes 8192 | tf_op jit(solution)/shard_map/all_to_all | solution.py:54
  58.6 0.8 fusion.22
  59.4 1.9 %fusion = f32[384]{0:T(512)S(1)} fusion(bf16[1,384,2048]{2,1,0:T(8,128)(2,1)} %param.9), kind=kLoop, calls=%fused_computation.2 | loop fusion | flops 2358912 | bytes 1574400 | tf_op jit(solution)/shard_map/reduce_sum | solution.py:13
  61.4 26.5 %all-gather.5.cloned.1.call-done = bf16[2,2048,512]{1,2,0:T(8,128)(2,1)} async-done(((bf16[2,2048,128]{1,2,0:T(8,128)(2,1)}), bf16[2,2048,512]{1,2,0:T(8,128)(2,1)}) %all-gather.5.cloned.1.call-update) | async-done | bytes 4194320 | tf_op jit(solution)/shard_map/all_gather | solution.py:40
  87.8 0.0 copy-done
  87.8 0.0 copy-done.6
  87.8 4.6 %fusion.10 = f32[2,384,512]{1,2,0:T(8,128)S(1)} fusion(bf16[2,2048,512]{1,2,0:T(8,128)(2,1)} %all-gather.5.cloned.1.call-done, bf16[1,384,2048]{2,1,0:T(8,128)(2,1)S(1)} %copy-done, f32[2048]{0:T(1024)S(1)} %copy-done.6, f32[384]{0:T(512)S(1)} %add_rsqrt_fusion.1), kind=kOutput, calls=%fused_computation.12 | convolution fusion | flops 1613758464 | bytes 7349760 | tf_op jit(solution)/shard_map/rd,kdc->krc/dot_general | solution.py:37
  92.5 0.0 copy-start.3
  92.5 0.1 slice.17
  92.5 0.0 copy-start.2
  92.5 0.0 copy-start.4
  92.6 0.3 copy.27
  92.8 0.0 copy-start.5
  92.8 0.1 multiply_reduce_fusion
  92.9 0.2 copy-done.3
  93.1 1.0 multiply_convert_fusion
  94.1 0.0 all-to-all-done.2
  94.1 3.5 %all-to-all-start = ((bf16[384,4,128]{2,0,1:T(8,128)(2,1)}), bf16[384,4,128]{2,0,1:T(8,128)(2,1)S(1)}, u32[]{:S(2)}, u32[]{:S(2)}) async-start(bf16[384,4,128]{2,0,1:T(8,128)(2,1)} %multiply_convert_fusion), calls=%async_computation | async-start | bytes 786432 | tf_op jit(solution)/shard_map/all_to_all | solution.py:52
  97.6 0.1 reshape.97
  97.8 0.9 copy.28
  98.7 6.3 %all-to-all-done = bf16[384,4,128]{2,0,1:T(8,128)(2,1)S(1)} async-done(((bf16[384,4,128]{2,0,1:T(8,128)(2,1)}), bf16[384,4,128]{2,0,1:T(8,128)(2,1)S(1)}, u32[]{:S(2)}, u32[]{:S(2)}) %all-to-all-start) | async-done | bytes 393248 | tf_op jit(solution)/shard_map/all_to_all | solution.py:52
  105.0 3.5 %all-to-all-start.1 = ((bf16[384,4,128]{2,0,1:T(8,128)(2,1)}), bf16[384,4,128]{2,0,1:T(8,128)(2,1)S(1)}, u32[]{:S(2)}, u32[]{:S(2)}) async-start(bf16[384,4,128]{2,0,1:T(8,128)(2,1)} %copy.28), calls=%async_computation.1 | async-start | bytes 786432 | tf_op jit(solution)/shard_map/all_to_all | solution.py:53
  108.5 0.0 copy-done.2
  108.5 0.3 fusion.17
  108.8 5.0 %reduce-window.6 = f32[4,12,128]{2,1,0:T(8,128)S(1)} reduce-window(f32[4,12,128]{2,1,0:T(8,128)S(1)} %reshape.89, f32[]{:T(128)} %constant.8.clone.1), window={size=1x1x128 pad=0_0x0_0x0_127}, to_apply=%region_3.4 | reduce-window | flops 780288 | bytes 49156 | tf_op jit(solution)/shard_map/reduce-window
  113.8 0.1 slice_reduce_fusion
  113.8 0.2 reduce-window.9
  114.0 0.1 slice.16
  114.1 0.1 add_bitcast_fusion
  114.2 1.6 %all-to-all-done.1 = bf16[384,4,128]{2,0,1:T(8,128)(2,1)S(1)} async-done(((bf16[384,4,128]{2,0,1:T(8,128)(2,1)}), bf16[384,4,128]{2,0,1:T(8,128)(2,1)S(1)}, u32[]{:S(2)}, u32[]{:S(2)}) %all-to-all-start.1) | async-done | bytes 393248 | tf_op jit(solution)/shard_map/all_to_all | solution.py:53
  115.8 0.3 multiply_reduce_fusion.1
  116.2 0.6 fusion.25
  116.8 0.7 copy.39
  117.5 0.7 copy.40
  (12 shorter events, 0.1 us)
Async XLA Ops:
  7.2 80.7 %copy-start = (bf16[1,384,2048]{2,1,0:T(8,128)(2,1)S(1)}, bf16[1,384,2048]{2,1,0:T(8,128)(2,1)}, u32[]{:S(2)}) copy-start(bf16[1,384,2048]{2,1,0:T(8,128)(2,1)} %param.9) | copy-start | bytes 4718596
  7.2 80.7 %copy-start.6 = (f32[2048]{0:T(1024)S(1)}, f32[2048]{0:T(1024)}, u32[]{:S(2)}) copy-start(f32[2048]{0:T(1024)} %param.10) | copy-start | bytes 24580
  7.2 45.6 %all-gather.3.cloned.1.call-start = ((), (), s32[]{:S(2)}) async-start(), calls=%async_computation.3 | async-start | bytes 1179648 | tf_op jit(solution)/shard_map/all_gather | solution.py:36
  9.9 77.9 %all-gather.5.cloned.1.call-start = ((), (), s32[]{:S(2)}) async-start(), calls=%async_computation.4 | async-start | bytes 5242880 | tf_op jit(solution)/shard_map/all_gather | solution.py:40
  55.3 38.8 %all-to-all-start.2 = ((bf16[4,2,192]{2,1,0:T(2,128)(2,1)}), bf16[4,2,192]{2,1,0:T(2,128)(2,1)S(1)}, u32[]{:S(2)}, u32[]{:S(2)}) async-start(bf16[4,2,192]{2,1,0:T(2,128)(2,1)} %reshape.96), calls=%async_computation.2 | async-start | bytes 8192 | tf_op jit(solution)/shard_map/all_to_all | solution.py:54
  92.5 0.7 copy-start.3
  92.5 15.9 %copy-start.2 = (bf16[1,4,128]{2,1,0:T(4,128)(2,1)S(1)}, bf16[1,4,128]{2,1,0:T(4,128)(2,1)}, u32[]{:S(2)}) copy-start(bf16[1,4,128]{2,1,0:T(4,128)(2,1)} %param.15) | copy-start | bytes 3076
  92.5 15.9 %copy-start.4 = (f32[128]{0:T(128)S(1)}, f32[128]{0:T(128)}, u32[]{:S(2)}) copy-start(f32[128]{0:T(128)} %param.16) | copy-start | bytes 1540
  92.8 23.3 %copy-start.5 = (f32[128]{0:T(128)S(1)}, f32[128]{0:T(128)}, u32[]{:S(2)}) copy-start(f32[128]{0:T(128)} %param.17) | copy-start | bytes 1540
  94.1 10.8 %all-to-all-start = ((bf16[384,4,128]{2,0,1:T(8,128)(2,1)}), bf16[384,4,128]{2,0,1:T(8,128)(2,1)S(1)}, u32[]{:S(2)}, u32[]{:S(2)}) async-start(bf16[384,4,128]{2,0,1:T(8,128)(2,1)} %multiply_convert_fusion), calls=%async_computation | async-start | bytes 786432 | tf_op jit(solution)/shard_map/all_to_all | solution.py:52
  97.7 20.6 %copy-start.1 = (bf16[4,1,384]{2,1,0:T(2,128)(2,1)}, bf16[4,1,384]{2,1,0:T(2,128)(2,1)S(1)}, u32[]{:S(2)}) copy-start(bf16[4,1,384]{2,1,0:T(2,128)(2,1)S(1)} %reshape.97) | copy-start | bytes 9220
  105.0 10.8 %all-to-all-start.1 = ((bf16[384,4,128]{2,0,1:T(8,128)(2,1)}), bf16[384,4,128]{2,0,1:T(8,128)(2,1)S(1)}, u32[]{:S(2)}, u32[]{:S(2)}) async-start(bf16[384,4,128]{2,0,1:T(8,128)(2,1)} %copy.28), calls=%async_computation.1 | async-start | bytes 786432 | tf_op jit(solution)/shard_map/all_to_all | solution.py:53
Sparse Core Ops, SparseCore 0:
  10.6 42.1 all-gather.2
  54.3 33.4 all-gather.4
where the time goes:
time: 126 us; the launch traced here: 125 us
  waiting for transfers between devices  77.2 us (61%)
  between operations  14.2 us (11%)
  other arithmetic  11.1 us (9%)
  starting transfers between devices  10.2 us (8%)
  local copies, waits for them, and re-layouts  7.15 us (6%)
  matrix products  5.2 us (4%)
    all_gather x1, waiting for transfers between devices, shards(): full_depth = lax.all_gather(stacked, 'sp', axis=1, tiled=True)  42.8 us
    all_gather x1, waiting for transfers between devices, shards(): lax.all_gather(full_depth, 'tp', axis=2, tiled=True)  26.5 us
    all_to_all x1, waiting for transfers between devices, shards(): lax.all_to_all(key_slots, 'tp', split_axis=1, concat_axis=0, tiled=True)  6.25 us
    another operation x2, other arithmetic  5.17 us
    unnamed x21, local copies, waits for them, and re-layouts  4.98 us
    dot_general x1, matrix products, shards(): jnp.einsum('rd,kdc->krc', normed, lax.all_gather(full_depth, 'tp', axis=2...  4.62 us
    all_to_all x1, starting transfers between devices, shards(): lax.all_to_all(key_slots, 'tp', split_axis=1, concat_axis=0, tiled=True)  3.46 us
    all_to_all x1, starting transfers between devices, shards(): lax.all_to_all(value_slots, 'tp', split_axis=1, concat_axis=0, tiled=True)  3.46 us
  transfers between devices with their start and end apart: 5, of which 4 were waited for; matrix products, arithmetic and copies ran while one was open for 14% of the time, Pallas kernels for 0%

commit v1 on v0

--- a/solution.py
+++ b/solution.py
@@ -5,6 +5,27 @@
 
 KVH = 4
 epsilon = 1e-06
+
+
+def in_order(blocks, dim):
+    blocks = jnp.moveaxis(blocks, 0, dim)
+    lengths = blocks.shape
+    return blocks.reshape(*lengths[:dim], lengths[dim] * lengths[dim + 1], *lengths[dim + 2 :])
+
+
+def collected_by_bits(value, axis):
+    size, here = (lax.axis_size(axis), lax.axis_index(axis))
+    blocks, bit = (value[None], 1)
+    while bit < size:
+        theirs = lax.ppermute(blocks, axis, [(i, i ^ bit) for i in range(size)])
+        low = here & bit == 0
+        blocks = jnp.concatenate([jnp.where(low, blocks, theirs), jnp.where(low, theirs, blocks)])
+        bit *= 2
+    return blocks
+
+
+def doubled_up(array, axis, dim):
+    return in_order(collected_by_bits(array, axis), dim)
 
 
 def row_norm(value_entries, scaling):
@@ -35,10 +56,7 @@
     stacked = jnp.stack((key_weight, value_weight), 0)
     full_depth = lax.all_gather(stacked, "sp", axis=1, tiled=True)
     projected = jnp.einsum(
-        "rd,kdc->krc",
-        normed,
-        lax.all_gather(full_depth, "tp", axis=2, tiled=True),
-        preferred_element_type=jnp.float32,
+        "rd,kdc->krc", normed, doubled_up(full_depth, "tp", 2), preferred_element_type=jnp.float32
     )
     key_rows = row_norm(projected[0].reshape(row_count, KVH, head_size), key_gain).astype(
         jnp.bfloat16

time: 126 us -> 156 us (1.24)
  waiting for transfers between devices: 77.2 us -> 95.2 us
  other arithmetic: 11.1 us -> 18.2 us
  local copies, waits for them, and re-layouts: 7.15 us -> 11 us
  starting transfers between devices: 10.2 us -> 11.8 us
    ppermute x0 -> x2, waiting for transfers between devices: none -> 42.3 us  [collected_by_bits(): theirs = lax.ppermute(blocks, axis, [(i, i ^ bit) for i in range(size)])]
    all_gather x1 -> x0, waiting for transfers between devices: 26.5 us -> none  [shards(): lax.all_gather(full_depth, 'tp', axis=2, tiled=True)]
    transpose x0 -> x1, local copies, waits for them, and re-layouts: none -> 6.51 us  [in_order(): blocks = jnp.moveaxis(blocks, 0, dim)]
    select_n x0 -> x2, other arithmetic: none -> 3.23 us  [collected_by_bits(): jnp.where(low, blocks, theirs)]
    transpose x0 -> x1, other arithmetic: none -> 2.29 us  [in_order(): blocks = jnp.moveaxis(blocks, 0, dim)]
    all_gather x1, waiting for transfers between devices: 42.8 us -> 45 us  [shards(): full_depth = lax.all_gather(stacked, 'sp', axis=1, tiled=True)]
    unnamed x21, local copies, waits for them, and re-layouts: 4.98 us -> 3.03 us
  transfers between devices with their start and end apart: 5 -> 6, of which waited for: 4 -> 5; matrix products, arithmetic and copies ran while one was open for 14% -> 18% of each run, Pallas kernels for 0% -> 0%
where the time goes in v1:
time: 156 us
  waiting for transfers between devices  95.2 us (61%)
  other arithmetic  18.2 us (12%)
  between operations  14.2 us (9%)
  starting transfers between devices  11.8 us (8%)
  local copies, waits for them, and re-layouts  11 us (7%)
  matrix products  5.2 us (3%)
    all_gather x1, waiting for transfers between devices, shards(): full_depth = lax.all_gather(stacked, 'sp', axis=1, tiled=True)  45 us
    ppermute x2, waiting for transfers between devices, collected_by_bits(): theirs = lax.ppermute(blocks, axis, [(i, i ^ bit) for i in range(size)])  42.3 us
    transpose x1, local copies, waits for them, and re-layouts, in_order(): blocks = jnp.moveaxis(blocks, 0, dim)  6.51 us
    all_to_all x1, waiting for transfers between devices, shards(): lax.all_to_all(key_slots, 'tp', split_axis=1, concat_axis=0, tiled=True)  6.25 us
    another operation x2, other arithmetic  5.17 us
    dot_general x1, matrix products, shards(): jnp.einsum('rd,kdc->krc', normed, doubled_up(full_depth, 'tp', 2), prefer...  4.62 us
    all_to_all x1, starting transfers between devices, shards(): lax.all_to_all(key_slots, 'tp', split_axis=1, concat_axis=0, tiled=True)  3.59 us
    all_to_all x1, starting transfers between devices, shards(): lax.all_to_all(value_slots, 'tp', split_axis=1, concat_axis=0, tiled=True)  3.46 us
  transfers between devices with their start and end apart: 6, of which 5 were waited for; matrix products, arithmetic and copies ran while one was open for 18% of the time, Pallas kernels for 0%

profile of v1, /device:TPU:0, one launch (start us, length us, event | category | flops | bytes accessed | tf_op | source)
XLA Modules:
  0.0 155.7 jit_solution(16078421419363230683)
XLA Ops:
  7.2 0.0 all-gather.2.cloned.1.call-start
  7.2 1.5 pad_maximum_fusion.1
  8.8 0.0 all-gather.2.cloned.1.call-update
  8.8 45.0 %all-gather.2.cloned.1.call-done = bf16[2,2048,128]{2,1,0:T(8,128)(2,1)} async-done(((bf16[2,256,128]{2,1,0:T(8,128)(2,1)}), bf16[2,2048,128]{2,1,0:T(8,128)(2,1)}) %all-gather.2.cloned.1.call-update) | async-done | bytes 1048592 | tf_op jit(solution)/shard_map/all_gather | solution.py:57
  53.7 0.0 collective-permute-start
  53.7 2.9 %collective-permute-done = bf16[1,2,2048,128]{3,2,1,0:T(8,128)(2,1)S(1)} collective-permute-done((bf16[1,2,2048,128]{3,2,1,0:T(8,128)(2,1)}, bf16[1,2,2048,128]{3,2,1,0:T(8,128)(2,1)S(1)}, u32[]{:S(2)}, u32[]{:S(2)}) %collective-permute-start) | collective-permute-done | bytes 1048608 | tf_op jit(solution)/shard_map/ppermute | solution.py:20
  56.6 1.4 broadcast_select_fusion.3
  58.0 0.0 copy-start.2
  58.0 0.0 copy-start.3
  58.0 1.5 pad_maximum_fusion
  59.5 1.5 collective-permute-start.1
  61.0 0.5 broadcast.82
  61.5 0.7 reduce.6
  62.2 0.7 reshape.113
  62.9 3.2 %all-to-all-start.2 = ((bf16[4,2,192]{2,1,0:T(2,128)(2,1)}), bf16[4,2,192]{2,1,0:T(2,128)(2,1)S(1)}, u32[]{:S(2)}, u32[]{:S(2)}) async-start(bf16[4,2,192]{2,1,0:T(2,128)(2,1)} %reshape.113), calls=%async_computation.2 | async-start | bytes 8192 | tf_op jit(solution)/shard_map/all_to_all | solution.py:72
  66.2 0.0 copy-done.3
  66.2 0.1 fusion.21
  66.3 1.8 %fusion = f32[384]{0:T(512)S(1)} fusion(bf16[1,384,2048]{2,1,0:T(8,128)(2,1)} %param.9), kind=kLoop, calls=%fused_computation.3 | loop fusion | flops 2358912 | bytes 1574400 | tf_op jit(solution)/shard_map/reduce_sum | solution.py:34
  68.1 39.5 %collective-permute-done.1 = bf16[2,2,2048,128]{3,2,1,0:T(8,128)(2,1)} collective-permute-done((bf16[2,2,2048,128]{3,2,1,0:T(8,128)(2,1)}, bf16[2,2,2048,128]{3,2,1,0:T(8,128)(2,1)}, u32[]{:S(2)}, u32[]{:S(2)}) %collective-permute-start.1) | collective-permute-done | bytes 2097184 | tf_op jit(solution)/shard_map/ppermute | solution.py:20
  107.5 1.9 %broadcast_select_fusion.1 = (bf16[2,2,2048,128]{3,2,1,0:T(8,128)(2,1)S(1)}, bf16[2,2,2048,128]{3,2,1,0:T(8,128)(2,1)S(1)}) fusion(bf16[2,2,2048,128]{3,2,1,0:T(8,128)(2,1)} %collective-permute-done.1, pred[]{:T(512)S(6)} %eq.6, bf16[1,2,2048,128]{3,2,1,0:T(8,128)(2,1)S(1)} %get-tuple-element.7, bf16[1,2,2048,128]{3,2,1,0:T(8,128)(2,1)S(1)} %get-tuple-element.6), kind=kLoop, calls=%fused_computation.10 | loop fusion | flops 3145728 | bytes 8388609 | tf_op jit(solution)/shard_map/jit(_where)/select_n | solution.py:22
  109.4 2.3 %maximum_bitcast_fusion = bf16[2,2048,4,128]{3,1,0,2:T(8,128)(2,1)} fusion(bf16[2,2,2048,128]{3,2,1,0:T(8,128)(2,1)S(1)} %get-tuple-element.5, bf16[2,2,2048,128]{3,2,1,0:T(8,128)(2,1)S(1)} %get-tuple-element.4), kind=kLoop, calls=%fused_computation | loop fusion | flops 2097152 | bytes 8388608 | tf_op jit(solution)/shard_map/transpose | solution.py:11
  111.7 6.5 %copy.22 = bf16[2,2048,4,128]{1,3,2,0:T(8,128)(2,1)} copy(bf16[2,2048,4,128]{3,1,0,2:T(8,128)(2,1)} %maximum_bitcast_fusion) | data formatting | bytes 8388608 | tf_op jit(solution)/shard_map/transpose | solution.py:11
  118.2 0.0 copy-done
  118.2 4.6 %fusion.9 = f32[2,384,512]{1,2,0:T(8,128)S(1)} fusion(bf16[2,2048,512]{1,2,0:T(8,128)(2,1)} %bitcast.69, bf16[1,384,2048]{2,1,0:T(8,128)(2,1)S(1)} %copy-done, f32[2048]{0:T(1024)S(1)} %copy-done.7, f32[384]{0:T(512)S(1)} %add_rsqrt_fusion.1), kind=kOutput, calls=%fused_computation.15 | convolution fusion | flops 1613758464 | bytes 7349760 | tf_op jit(solution)/shard_map/rd,kdc->krc/dot_general | solution.py:58
  122.8 0.0 copy-start.4
  122.9 0.1 slice.17
  122.9 0.3 copy.23
  123.2 0.1 multiply_reduce_fusion
  123.3 0.2 copy-done.4
  123.5 1.0 multiply_convert_fusion
  124.5 0.0 all-to-all-done.2
  124.5 3.6 %all-to-all-start = ((bf16[384,4,128]{2,0,1:T(8,128)(2,1)}), bf16[384,4,128]{2,0,1:T(8,128)(2,1)S(1)}, u32[]{:S(2)}, u32[]{:S(2)}) async-start(bf16[384,4,128]{2,0,1:T(8,128)(2,1)} %multiply_convert_fusion), calls=%async_computation | async-start | bytes 786432 | tf_op jit(solution)/shard_map/all_to_all | solution.py:70
  128.1 0.1 reshape.114
  128.3 0.9 copy.24
  129.3 6.3 %all-to-all-done = bf16[384,4,128]{2,0,1:T(8,128)(2,1)S(1)} async-done(((bf16[384,4,128]{2,0,1:T(8,128)(2,1)}), bf16[384,4,128]{2,0,1:T(8,128)(2,1)S(1)}, u32[]{:S(2)}, u32[]{:S(2)}) %all-to-all-start) | async-done | bytes 393248 | tf_op jit(solution)/shard_map/all_to_all | solution.py:70
  135.5 3.5 %all-to-all-start.1 = ((bf16[384,4,128]{2,0,1:T(8,128)(2,1)}), bf16[384,4,128]{2,0,1:T(8,128)(2,1)S(1)}, u32[]{:S(2)}, u32[]{:S(2)}) async-start(bf16[384,4,128]{2,0,1:T(8,128)(2,1)} %copy.24), calls=%async_computation.1 | async-start | bytes 786432 | tf_op jit(solution)/shard_map/all_to_all | solution.py:71
  139.0 0.3 fusion.16
  139.3 5.0 %reduce-window.6 = f32[4,12,128]{2,1,0:T(8,128)S(1)} reduce-window(f32[4,12,128]{2,1,0:T(8,128)S(1)} %reshape.107, f32[]{:T(128)} %constant.13.clone.1), window={size=1x1x128 pad=0_0x0_0x0_127}, to_apply=%region_3.4 | reduce-window | flops 780288 | bytes 49156 | tf_op jit(solution)/shard_map/reduce-window
  144.3 0.1 slice_reduce_fusion
  144.4 0.2 reduce-window.9
  144.6 0.1 slice.16
  144.6 0.1 add_bitcast_fusion
  144.7 1.7 %all-to-all-done.1 = bf16[384,4,128]{2,0,1:T(8,128)(2,1)S(1)} async-done(((bf16[384,4,128]{2,0,1:T(8,128)(2,1)}), bf16[384,4,128]{2,0,1:T(8,128)(2,1)S(1)}, u32[]{:S(2)}, u32[]{:S(2)}) %all-to-all-start.1) | async-done | bytes 393248 | tf_op jit(solution)/shard_map/all_to_all | solution.py:71
  146.4 0.3 multiply_reduce_fusion.1
  146.7 0.6 fusion.24
  147.3 0.7 copy.35
  148.1 0.0 copy-done.1
  148.1 0.7 copy.36
  (18 shorter events, 0.2 us)
Async XLA Ops:
  7.2 46.6 %all-gather.2.cloned.1.call-start = ((), (), s32[]{:S(2)}) async-start(), calls=%async_computation.3 | async-start | bytes 1179648 | tf_op jit(solution)/shard_map/all_gather | solution.py:57
  53.7 2.9 %collective-permute-start = (bf16[1,2,2048,128]{3,2,1,0:T(8,128)(2,1)}, bf16[1,2,2048,128]{3,2,1,0:T(8,128)(2,1)S(1)}, u32[]{:S(2)}, u32[]{:S(2)}) collective-permute-start(bf16[1,2,2048,128]{3,2,1,0:T(8,128)(2,1)} %bitcast.75), channel_id=1, source_target_pairs={{0,1},{1,0},{2,3},{3,2},{4,5},{5,4},{6,7},{7,6},{8,9},{9,8},{10,11... | collective-permute-start | bytes 3145736 | tf_op jit(solution)/shard_map/ppermute | solution.py:20
  58.0 3.0 %copy-start.2 = (bf16[1,4,384]{2,1,0:T(4,128)(2,1)S(1)}, bf16[1,4,384]{2,1,0:T(4,128)(2,1)}, u32[]{:S(2)}) copy-start(bf16[1,4,384]{2,1,0:T(4,128)(2,1)} %param.14) | copy-start | bytes 9220
  58.0 8.2 %copy-start.3 = (bf16[1,4,128]{2,1,0:T(4,128)(2,1)S(1)}, bf16[1,4,128]{2,1,0:T(4,128)(2,1)}, u32[]{:S(2)}) copy-start(bf16[1,4,128]{2,1,0:T(4,128)(2,1)} %param.15) | copy-start | bytes 3076
  59.5 48.0 %collective-permute-start.1 = (bf16[2,2,2048,128]{3,2,1,0:T(8,128)(2,1)}, bf16[2,2,2048,128]{3,2,1,0:T(8,128)(2,1)}, u32[]{:S(2)}, u32[]{:S(2)}) collective-permute-start(bf16[2,2,2048,128]{3,2,1,0:T(8,128)(2,1)} %pad_maximum_fusion), channel_id=1, source_target_pairs={{0,2},{1,3},{2,0},{3,1},{4,6},{5,7},{6,4},{7,5},{8,10},{9,11},{10,... | collective-permute-start | bytes 6291464 | tf_op jit(solution)/shard_map/ppermute | solution.py:20
  62.9 61.6 %all-to-all-start.2 = ((bf16[4,2,192]{2,1,0:T(2,128)(2,1)}), bf16[4,2,192]{2,1,0:T(2,128)(2,1)S(1)}, u32[]{:S(2)}, u32[]{:S(2)}) async-start(bf16[4,2,192]{2,1,0:T(2,128)(2,1)} %reshape.113), calls=%async_computation.2 | async-start | bytes 8192 | tf_op jit(solution)/shard_map/all_to_all | solution.py:72
  111.7 6.5 %copy-start = (bf16[1,384,2048]{2,1,0:T(8,128)(2,1)S(1)}, bf16[1,384,2048]{2,1,0:T(8,128)(2,1)}, u32[]{:S(2)}) copy-start(bf16[1,384,2048]{2,1,0:T(8,128)(2,1)} %param.9) | copy-start | bytes 4718596
  111.7 6.5 %copy-start.7 = (f32[2048]{0:T(1024)S(1)}, f32[2048]{0:T(1024)}, u32[]{:S(2)}) copy-start(f32[2048]{0:T(1024)} %param.10) | copy-start | bytes 24580
  122.8 0.7 copy-start.4
  123.5 15.5 %copy-start.5 = (f32[128]{0:T(128)S(1)}, f32[128]{0:T(128)}, u32[]{:S(2)}) copy-start(f32[128]{0:T(128)} %param.16) | copy-start | bytes 1540
  124.5 22.2 %copy-start.6 = (f32[128]{0:T(128)S(1)}, f32[128]{0:T(128)}, u32[]{:S(2)}) copy-start(f32[128]{0:T(128)} %param.17) | copy-start | bytes 1540
  124.5 11.0 %all-to-all-start = ((bf16[384,4,128]{2,0,1:T(8,128)(2,1)}), bf16[384,4,128]{2,0,1:T(8,128)(2,1)S(1)}, u32[]{:S(2)}, u32[]{:S(2)}) async-start(bf16[384,4,128]{2,0,1:T(8,128)(2,1)} %multiply_convert_fusion), calls=%async_computation | async-start | bytes 786432 | tf_op jit(solution)/shard_map/all_to_all | solution.py:70
  128.2 19.8 %copy-start.1 = (bf16[4,1,384]{2,1,0:T(2,128)(2,1)}, bf16[4,1,384]{2,1,0:T(2,128)(2,1)S(1)}, u32[]{:S(2)}) copy-start(bf16[4,1,384]{2,1,0:T(2,128)(2,1)S(1)} %reshape.114) | copy-start | bytes 9220
  135.5 10.8 %all-to-all-start.1 = ((bf16[384,4,128]{2,0,1:T(8,128)(2,1)}), bf16[384,4,128]{2,0,1:T(8,128)(2,1)S(1)}, u32[]{:S(2)}, u32[]{:S(2)}) async-start(bf16[384,4,128]{2,0,1:T(8,128)(2,1)} %copy.24), calls=%async_computation.1 | async-start | bytes 786432 | tf_op jit(solution)/shard_map/all_to_all | solution.py:71
Sparse Core Ops, SparseCore 0:
  10.7 42.9 all-gather.1
